TPU v7x, 32 devices: a whole 2x2x4 slice. The times are simulated.
32 devices in a mesh: dp: 4 (over y, x), kv: 4 (over z), tp: 2 (over core).
Axes of the slice: x: 2, y: 2, z: 4, core: 2. Of those that a mesh axis runs over, the one named last changes fastest.
Arguments:
- tokens: bfloat16 [64, 4096], P('dp', 'kv'), may hold values from -51 to 51
- norm_gain: float32 [4096], P('kv'), may hold values from 0.1 to 1.9
- w_query: bfloat16 [4096, 2048], P('kv', 'tp'), may hold values from -0.09375 to 0.09375
- lambda_head: float32 [16], P('tp'), may hold values from 0.3 to 0.8
- head_gain: float32 [128], replicated, may hold values from 0.1 to 1.9
- w_out: bfloat16 [2048, 4096], P('tp', 'kv'), may hold values from -0.125 to 0.125
- rotated_key_cache: bfloat16 [64, 1024, 128], P('dp', 'kv'), may hold values from -540 to 540, as said below
- value_cache: bfloat16 [64, 1024, 128], P('dp', 'kv'), may hold values from -6 to 6
- lengths: int32 [64], P('dp'), may hold values from 256 to 1024
Outputs:
- mixed: bfloat16 [64, 4096], P('dp', ('kv', 'tp'))
Inputs may be any that keep to these rules, and one draw needn't show every extreme that they name: `rotated_key_cache`: keys have an order-one typical size. The new token is the last filled position, lengths - 1.
All inputs are finite; a program needn't handle non-finite values.
Results may differ from a plain program's by a relative error of at most 0.0112.
Values may be sent and summed in bfloat16 or wider, within the bound.
No kernel may reach another device: no remote copies, remote signals or barrier semaphores. Data moves between devices by JAX's collectives and lax.ppermute only.
A program may use at most 64 MiB of HBM per device.

v0:
```python
import jax
import jax.numpy as jnp
from jax import lax
from jax.sharding import PartitionSpec as P

D = 4096
HEAD_FEATURES = 64
VALUE_DIM = 128
EPS = 1e-05


def combined_all(part, axis, combine):
    gathered = jax.tree.map(lambda a: lax.all_gather(a, axis), part)

    def take(source):
        return jax.tree.map(lambda a: lax.dynamic_index_in_dim(a, source, 0, False), gathered)

    return lax.fori_loop(
        1, lax.axis_size(axis), lambda source, state: combine(state, take(source)), take(0)
    )


def rotate_query(query, position):
    half_dim = query.shape[-1] // 2
    frequency = 1.0 / 10000.0 ** (jnp.arange(half_dim, dtype=jnp.float32) / half_dim)
    angles = position[:, None] * frequency[None, :]
    cosine_table = jnp.concatenate([jnp.cos(angles), jnp.cos(angles)], -1)[:, None, None, :]
    sine_table = jnp.concatenate([jnp.sin(angles), jnp.sin(angles)], -1)[:, None, None, :]
    first_half = query[..., :half_dim]
    second_half = query[..., half_dim:]
    turned = jnp.concatenate([-second_half, first_half], -1)
    return query * cosine_table + turned * sine_table


def finish(numerators, totals, lambdas, head_gain):
    averaged = numerators / totals[..., None]
    head_result = averaged[..., 0, :] - lambdas[..., None] * averaged[..., 1, :]
    factor = lax.rsqrt(jnp.mean(head_result * head_result, -1, keepdims=True) + EPS)
    return (head_result * factor * head_gain).astype(jnp.bfloat16)


def combine_blocks(earlier, later):
    top = jnp.maximum(earlier[0], later[0])
    first_factor = jnp.exp(earlier[0] - top)
    second_factor = jnp.exp(later[0] - top)
    totals = earlier[1] * first_factor + later[1] * second_factor
    numerators = earlier[2] * first_factor[..., None] + later[2] * second_factor[..., None]
    return (top, totals, numerators)


def on_device(
    tokens,
    norm_gain,
    w_query,
    lambda_head,
    head_gain,
    w_out,
    rotated_key_cache,
    value_cache,
    lengths,
):
    seq_count = tokens.shape[0]
    head_count = lambda_head.shape[0]
    pos_count = rotated_key_cache.shape[1]
    widened = tokens.astype(jnp.float32)
    squares = jnp.sum(widened * widened, -1)
    scaled_in = (widened * norm_gain).astype(jnp.bfloat16)
    partial_query = jnp.dot(scaled_in, w_query, preferred_element_type=jnp.float32)
    squares = lax.psum(squares, "kv")
    raw_query = lax.psum(partial_query, "kv")
    scale_rows = lax.rsqrt(squares / D + EPS)
    shaped = (raw_query * scale_rows[:, None]).reshape(seq_count, head_count, 2, HEAD_FEATURES)
    query = rotate_query(shaped, (lengths - 1).astype(jnp.float32))
    keys = rotated_key_cache.reshape(seq_count, pos_count, 2, HEAD_FEATURES)
    score_rows = jnp.einsum(
        "bhmd,bpmd->bhmp",
        query,
        keys,
        preferred_element_type=jnp.float32,
        precision=lax.Precision.HIGHEST,
    ) * HEAD_FEATURES ** (-0.5)
    position_list = lax.axis_index("kv") * pos_count + jnp.arange(pos_count, dtype=jnp.int32)
    valid = (position_list[None, :] < lengths[:, None])[:, None, None, :]
    masked = jnp.where(valid, score_rows, -1e30)
    maxima = jnp.max(masked, -1)
    weights = jnp.where(valid, jnp.exp(masked - maxima[..., None]), 0.0)
    totals = jnp.sum(weights, -1)
    numerators = jnp.einsum(
        "bhmp,bpv->bhmv",
        weights.astype(jnp.bfloat16),
        value_cache,
        preferred_element_type=jnp.float32,
    )
    merged = combined_all((maxima, totals, numerators), "kv", combine_blocks)
    normed = finish(merged[2], merged[1], lambda_head[None, :], head_gain).reshape(
        seq_count, head_count * VALUE_DIM
    )
    projected = jnp.dot(normed, w_out, preferred_element_type=jnp.float32)
    return lax.psum_scatter(projected, "tp", scatter_dimension=1, tiled=True).astype(jnp.bfloat16)


def solution(mesh):
    in_specs = (
        P("dp", "kv"),
        P("kv"),
        P("kv", "tp"),
        P("tp"),
        P(),
        P("tp", "kv"),
        P("dp", "kv", None),
        P("dp", "kv", None),
        P("dp"),
    )
    out_specs = P("dp", ("kv", "tp"))
    return jax.shard_map(
        on_device, mesh=mesh, in_specs=in_specs, out_specs=out_specs, check_vma=False
    )
```

profile of v0, /device:TPU:0, one launch (start us, length us, event | category | flops | bytes accessed | tf_op | source)
XLA Modules:
  0.0 114.8 jit_solution(7172652897911853085)
XLA Ops:
  6.5 0.0 copy-start
  6.5 0.0 copy-start.1
  6.5 0.0 copy-start.4
  6.5 0.0 copy-start.2
  6.5 0.0 copy-start.3
  6.5 0.0 all-reduce.2.cloned.1.call-start
  6.6 1.5 %copy-done = bf16[1024,1024]{1,0:T(8,128)(2,1)S(1)} copy-done((bf16[1024,1024]{1,0:T(8,128)(2,1)S(1)}, bf16[1024,1024]{1,0:T(8,128)(2,1)}, u32[]{:S(2)}) %copy-start) | copy-done | bytes 2097176
  8.1 1.8 %fusion.28 = f32[16,1024]{1,0:T(8,128)} fusion(bf16[1024,1024]{1,0:T(8,128)(2,1)S(1)} %copy-done, bf16[16,1024]{1,0:T(8,128)(2,1)} %param.11, f32[1024]{0:T(1024)} %param.12), kind=kOutput, calls=%fused_computation.41 | convolution fusion | flops 33603584 | bytes 2199552 | tf_op jit(solution)/shard_map/dot_general | solution.py:68
  9.9 0.0 all-reduce.2.cloned.1.call-update
  9.9 0.0 reduce-scatter.2.cloned.1.call-start
  10.0 0.0 copy-done.1
  10.0 0.1 fusion.20
  10.1 0.0 copy-done.4
  10.1 13.5 %psum.15 = f32[16]{0:T(128)S(1)} all-reduce(f32[16]{0:T(128)S(1)} %fusion.20), channel_id=1, replica_groups=mesh['dp'=4,'kv'=4,'tp'=2] {'kv'}, use_global_device_ids=true, to_apply=%region_2.0 | all-reduce | flops 16 | bytes 128 | tf_op jit(solution)/shard_map/psum | solution.py:69
  23.6 0.1 broadcast_compare_fusion
  23.7 1.5 %copy.41 = bf16[16,256,128]{1,2,0:T(8,128)(2,1)S(1)} copy(bf16[16,256,128]{2,1,0:T(8,128)(2,1)} %param.17) | data formatting | bytes 2097152 | tf_op args[6]
  25.2 0.1 multiply_cosine_fusion
  25.3 0.0 copy-done.2
  25.3 0.0 copy-done.3
  25.3 0.1 broadcast_bitcast_fusion
  25.4 0.1 pad_maximum_fusion
  25.5 21.6 %all-reduce.2.cloned.1.call-done = f32[16,1024]{1,0:T(8,128)} async-done(((f32[16,1024]{1,0:T(8,128)}), f32[16,1024]{1,0:T(8,128)}) %all-reduce.2.cloned.1.call-update) | async-done | bytes 65552 | tf_op jit(solution)/shard_map/psum | solution.py:70
  47.1 0.9 broadcast_multiply_fusion
  48.0 0.1 reshape.64
  48.2 0.0 copy-start.5
  48.2 0.1 slice_negate_fusion
  48.3 0.7 fusion.37
  49.0 13.2 %all-gather = f32[64,8,2]{1,2,0:T(2,128)S(1)} all-gather(f32[16,8,2]{1,2,0:T(2,128)S(1)} %get-tuple-element.230), channel_id=2, replica_groups=mesh['dp'=4,'kv'=4,'tp'=2] {'kv'}, dimensions={0}, use_global_device_ids=true | all-gather | bytes 5120 | tf_op jit(solution)/shard_map/all_gather | solution.py:13
  62.1 0.2 fusion.9
  62.4 0.0 copy-done.5
  62.4 0.3 fusion.6
  62.7 15.8 %all-gather.2 = f32[64,8,2,128]{3,1,2,0:T(8,128)S(1)} all-gather(f32[16,8,2,128]{3,1,2,0:T(8,128)S(1)} %fusion.6), channel_id=4, replica_groups=mesh['dp'=4,'kv'=4,'tp'=2] {'kv'}, dimensions={0}, use_global_device_ids=true | all-gather | bytes 655360 | tf_op jit(solution)/shard_map/all_gather | solution.py:13
  78.5 0.1 copy.46
  78.5 13.1 %all-gather.1 = f32[64,8,2]{1,2,0:T(2,128)S(1)} all-gather(f32[16,8,2]{1,2,0:T(2,128)S(1)} %fusion.9), channel_id=3, replica_groups=mesh['dp'=4,'kv'=4,'tp'=2] {'kv'}, dimensions={0}, use_global_device_ids=true | all-gather | bytes 5120 | tf_op jit(solution)/shard_map/all_gather | solution.py:13
  91.7 0.1 copy.48
  91.8 0.1 copy.45
  91.8 0.1 copy.47
  91.9 0.1 copy.44
  92.0 3.4 %while.19 = (s32[]{:T(128)}, f32[16,8,2]{0,2,1:T(2,128)S(1)}, f32[16,8,2]{0,2,1:T(2,128)S(1)}, f32[16,8,2,128]{3,2,1,0:T(2,128)S(1)}, f32[4,16,8,2]{1,3,2,0:T(2,...) while((s32[]{:T(128)}, f32[16,8,2]{0,2,1:T(2,128)S(1)}, ...), condition=%wide.region_6.7_spmd, body=%wide.region_5.6_spmd.sunk | while | flops 99845 | bytes 669847 | solution.py:18
  92.1 0.1 copy.83
  92.2 0.1 copy.84
  92.3 0.8 fusion.44
  93.2 0.1 copy.83
  93.3 0.1 copy.84
  93.5 0.8 fusion.44
  94.3 0.1 copy.83
  94.5 0.1 copy.84
  94.6 0.8 fusion.44
  95.4 0.1 copy.50
  95.5 0.2 broadcast_divide_fusion
  95.8 0.2 slice_reduce_fusion
  96.0 0.2 multiply_reduce_fusion
  96.2 0.1 mul.196
  96.3 2.6 %fusion.26 = f32[16,1024]{1,0:T(8,128)} fusion(bf16[1024,1024]{1,0:T(8,128)(2,1)} %param.16, f32[2,8,8,128]{3,2,1,0:T(8,128)S(1)} %bitcast.72, f32[2,8,8,128]{3,2,1,0:T(8,128)S(1)} %bitcast.71, f32[2,8,8,128]{3,2,1,0:T(8,128)S(1)} %bitcast.68, f32[1024]{0:T(1024)S(1)} %get-tuple-element.234, f32[1024]{0:T(1024)S(1)} %get-tuple-element.235), kind=kOutput, calls=%fused_computation.40 | convolution fusion | flops 33636352 | bytes 2367488 | tf_op jit(solution)/shard_map/dot_general | solution.py:98
  98.9 0.0 reduce-scatter.2.cloned.1.call-update
  98.9 7.8 %reduce-scatter.2.cloned.1.call-done = f32[16,512]{1,0:T(8,128)} async-done(((f32[16,1024]{1,0:T(8,128)}), f32[16,512]{1,0:T(8,128)}) %reduce-scatter.2.cloned.1.call-update) | async-done | bytes 32784 | tf_op jit(solution)/shard_map/reduce_scatter | solution.py:99
  106.6 1.4 %convert_element_type.24 = bf16[16,512]{1,0:T(8,128)(2,1)} convert(f32[16,512]{1,0:T(8,128)} %reduce-scatter.2.cloned.1.call-done) | non-fusion elementwise | flops 8192 | bytes 49152 | tf_op jit(solution)/shard_map/convert_element_type | solution.py:99
  (15 shorter events, 0.2 us)
Async XLA Ops:
  6.5 1.6 %copy-start = (bf16[1024,1024]{1,0:T(8,128)(2,1)S(1)}, bf16[1024,1024]{1,0:T(8,128)(2,1)}, u32[]{:S(2)}) copy-start(bf16[1024,1024]{1,0:T(8,128)(2,1)} %param.13) | copy-start | bytes 6291460
  6.5 3.4 %copy-start.1 = (bf16[16,1024]{1,0:T(8,128)(2,1)S(1)}, bf16[16,1024]{1,0:T(8,128)(2,1)}, u32[]{:S(2)}) copy-start(bf16[16,1024]{1,0:T(8,128)(2,1)} %param.11) | copy-start | bytes 98308
  6.5 3.6 %copy-start.4 = (s32[16]{0:T(128)S(1)}, s32[16]{0:T(128)}, u32[]{:S(2)}) copy-start(s32[16]{0:T(128)} %param.19) | copy-start | bytes 196
  6.5 18.8 %copy-start.2 = (f32[8]{0:T(128)S(1)}, f32[8]{0:T(128)}, u32[]{:S(2)}) copy-start(f32[8]{0:T(128)} %param.14) | copy-start | bytes 100
  6.5 18.8 %copy-start.3 = (f32[128]{0:T(128)S(1)}, f32[128]{0:T(128)}, u32[]{:S(2)}) copy-start(f32[128]{0:T(128)} %param.15) | copy-start | bytes 1540
  6.5 40.6 %all-reduce.2.cloned.1.call-start = ((), (), s32[]{:S(2)}) async-start(), calls=%async_computation.1 | async-start | bytes 131072 | tf_op jit(solution)/shard_map/psum | solution.py:70
  9.9 96.7 %reduce-scatter.2.cloned.1.call-start = ((), (), s32[]{:S(2)}) async-start(), calls=%async_computation.2 | async-start | bytes 98304 | tf_op jit(solution)/shard_map/reduce_scatter | solution.py:99
  48.2 14.2 %copy-start.5 = (bf16[16,256,128]{2,1,0:T(8,128)(2,1)S(1)}, bf16[16,256,128]{2,1,0:T(8,128)(2,1)}, u32[]{:S(2)}) copy-start(bf16[16,256,128]{2,1,0:T(8,128)(2,1)} %param.18) | copy-start | bytes 3145732
Sparse Core Ops, SparseCore 0:
  10.0 37.0 all-reduce.1
  99.0 7.5 reduce-scatter.1
where the time goes:
time: 115 us
  blocking collectives  55.5 us (48%)
  waiting for transfers between devices  29.4 us (26%)
  between operations  13.6 us (12%)
  other arithmetic  5.9 us (5%)
  matrix products  5.38 us (5%)
  local copies, waits for them, and re-layouts  4.94 us (4%)
    all_gather x3, blocking collectives, combined_all(): gathered = jax.tree.map(lambda a: lax.all_gather(a, axis), part)  42 us
    psum x1, waiting for transfers between devices, on_device(): raw_query = lax.psum(partial_query, 'kv')  21.6 us
    psum x1, blocking collectives, on_device(): squares = lax.psum(squares, 'kv')  13.5 us
    reduce_scatter x1, waiting for transfers between devices, on_device(): lax.psum_scatter(projected, 'tp', scatter_dimension=1, tiled=True)  7.75 us
    unnamed x13, local copies, waits for them, and re-layouts  3.04 us
    dot_general x1, matrix products, on_device(): projected = jnp.dot(normed, w_out, preferred_element_type=jnp.float32)  2.61 us
    add x3, other arithmetic, combine_blocks(): earlier[2] * first_factor[..., None] + later[2] * second_factor[..., None]  2.39 us
  transfers between devices with their start and end apart: 2, of which 2 were waited for; matrix products, arithmetic and copies ran while one was open for 2% of the time, Pallas kernels for 0%

commit v1 on v0

--- a/solution.py
+++ b/solution.py
@@ -67,7 +67,7 @@
     scaled_in = (widened * norm_gain).astype(jnp.bfloat16)
     partial_query = jnp.dot(scaled_in, w_query, preferred_element_type=jnp.float32)
     squares = lax.psum(squares, "kv")
-    raw_query = lax.psum(partial_query, "kv")
+    raw_query = jnp.sum(lax.all_gather(partial_query, "kv"), 0)
     scale_rows = lax.rsqrt(squares / D + EPS)
     shaped = (raw_query * scale_rows[:, None]).reshape(seq_count, head_count, 2, HEAD_FEATURES)
     query = rotate_query(shaped, (lengths - 1).astype(jnp.float32))

time: 115 us -> 104 us (0.904)
  waiting for transfers between devices: 29.4 us -> 5.95 us
  blocking collectives: 55.5 us -> 69.4 us
    psum x1 -> x0, waiting for transfers between devices: 21.6 us -> none  [on_device(): raw_query = lax.psum(partial_query, 'kv')]
    all_gather x0 -> x1, blocking collectives: none -> 15.6 us  [on_device(): raw_query = jnp.sum(lax.all_gather(partial_query, 'kv'), 0)]
    reduce_scatter x1, waiting for transfers between devices: 7.75 us -> 5.93 us  [on_device(): lax.psum_scatter(projected, 'tp', scatter_dimension=1, tiled=True)]
    psum x1, blocking collectives: 13.5 us -> 12.3 us  [on_device(): squares = lax.psum(squares, 'kv')]
    unnamed x13 -> x11, local copies, waits for them, and re-layouts: 3.04 us -> 2.06 us
  transfers between devices with their start and end apart: 2 -> 1, of which waited for: 2 -> 1; matrix products, arithmetic and copies ran while one was open for 2% -> 0% of each run, Pallas kernels for 0% -> 0%
where the time goes in v1:
time: 104 us
  blocking collectives  69.4 us (67%)
  between operations  13.6 us (13%)
  other arithmetic  6.37 us (6%)
  waiting for transfers between devices  5.95 us (6%)
  matrix products  4.68 us (4%)
  local copies, waits for them, and re-layouts  3.95 us (4%)
    all_gather x3, blocking collectives, combined_all(): gathered = jax.tree.map(lambda a: lax.all_gather(a, axis), part)  41.4 us
    all_gather x1, blocking collectives, on_device(): raw_query = jnp.sum(lax.all_gather(partial_query, 'kv'), 0)  15.6 us
    psum x1, blocking collectives, on_device(): squares = lax.psum(squares, 'kv')  12.3 us
    reduce_scatter x1, waiting for transfers between devices, on_device(): lax.psum_scatter(projected, 'tp', scatter_dimension=1, tiled=True)  5.93 us
    dot_general x1, matrix products, on_device(): projected = jnp.dot(normed, w_out, preferred_element_type=jnp.float32)  2.61 us
    add x3, other arithmetic, combine_blocks(): earlier[2] * first_factor[..., None] + later[2] * second_factor[..., None]  2.38 us
  transfers between devices with their start and end apart: 1, of which 1 were waited for; matrix products, arithmetic and copies ran while one was open for 0% of the time, Pallas kernels for 0%

profile of v1, /device:TPU:0, one launch (start us, length us, event | category | flops | bytes accessed | tf_op | source)
XLA Modules:
  0.0 103.9 jit_solution(15373554398320479739)
XLA Ops:
  6.5 0.0 copy-start
  6.5 0.0 copy-start.3
  6.5 0.0 reduce-scatter.2.cloned.1.call-start
  6.6 1.0 fusion.17
  7.6 0.6 copy-done
  8.1 1.1 %fusion.23 = f32[16,1024]{1,0:T(8,128)S(1)} fusion(bf16[1024,1024]{1,0:T(8,128)(2,1)S(1)} %copy-done, bf16[16,1024]{1,0:T(8,128)(2,1)} %param.11, f32[1024]{0:T(1024)} %param.12), kind=kOutput, calls=%fused_computation.38 | convolution fusion | flops 33603584 | bytes 2199552 | tf_op jit(solution)/shard_map/dot_general | solution.py:68
  9.3 15.6 %all-gather = f32[64,1024]{1,0:T(8,128)S(1)} all-gather(f32[16,1024]{1,0:T(8,128)S(1)} %fusion.23), channel_id=2, replica_groups=mesh['dp'=4,'kv'=4,'tp'=2] {'kv'}, dimensions={0}, use_global_device_ids=true | all-gather | bytes 327680 | tf_op jit(solution)/shard_map/all_gather | solution.py:70
  25.0 0.1 reduce_sum.39
  25.1 12.3 %psum.7 = f32[16]{0:T(128)S(1)} all-reduce(f32[16]{0:T(128)S(1)} %fusion.17), channel_id=1, replica_groups=mesh['dp'=4,'kv'=4,'tp'=2] {'kv'}, use_global_device_ids=true, to_apply=%region_2.0 | all-reduce | flops 16 | bytes 128 | tf_op jit(solution)/shard_map/psum | solution.py:69
  37.4 0.1 broadcast_multiply_fusion
  37.5 0.2 slice_negate_fusion
  37.7 0.0 copy-done.3
  37.8 0.1 broadcast_compare_fusion
  37.8 1.5 %copy.33 = bf16[16,256,128]{1,2,0:T(8,128)(2,1)S(1)} copy(bf16[16,256,128]{2,1,0:T(8,128)(2,1)} %param.17) | data formatting | bytes 2097152 | tf_op args[6]
  39.3 0.0 copy-start.4
  39.3 0.1 multiply_cosine_fusion
  39.5 0.1 pad_maximum_fusion
  39.5 0.2 fusion.11
  39.8 0.6 fusion.30
  40.4 13.3 %all-gather.1 = f32[64,8,2]{1,2,0:T(2,128)S(1)} all-gather(f32[16,8,2]{1,2,0:T(2,128)S(1)} %get-tuple-element.230), channel_id=3, replica_groups=mesh['dp'=4,'kv'=4,'tp'=2] {'kv'}, dimensions={0}, use_global_device_ids=true | all-gather | bytes 5120 | tf_op jit(solution)/shard_map/all_gather | solution.py:13
  53.7 0.2 fusion.9
  54.0 0.0 copy-done.4
  54.0 0.3 fusion.6
  54.3 14.9 %all-gather.3 = f32[64,8,2,128]{3,1,2,0:T(8,128)S(1)} all-gather(f32[16,8,2,128]{3,1,2,0:T(8,128)S(1)} %fusion.6), channel_id=5, replica_groups=mesh['dp'=4,'kv'=4,'tp'=2] {'kv'}, dimensions={0}, use_global_device_ids=true | all-gather | bytes 655360 | tf_op jit(solution)/shard_map/all_gather | solution.py:13
  69.2 0.1 copy.39
  69.3 13.1 %all-gather.2 = f32[64,8,2]{1,2,0:T(2,128)S(1)} all-gather(f32[16,8,2]{1,2,0:T(2,128)S(1)} %fusion.9), channel_id=4, replica_groups=mesh['dp'=4,'kv'=4,'tp'=2] {'kv'}, dimensions={0}, use_global_device_ids=true | all-gather | bytes 5120 | tf_op jit(solution)/shard_map/all_gather | solution.py:13
  82.4 0.1 copy.41
  82.5 0.1 copy.38
  82.6 0.1 copy.40
  82.7 0.1 copy.37
  82.8 0.0 copy-start.1
  82.8 0.0 copy-start.2
  82.8 3.4 %while.19 = (s32[]{:T(128)}, f32[16,8,2]{0,2,1:T(2,128)S(1)}, f32[16,8,2]{0,2,1:T(2,128)S(1)}, f32[16,8,2,128]{3,2,1,0:T(2,128)S(1)}, f32[4,16,8,2]{1,3,2,0:T(2,...) while((s32[]{:T(128)}, f32[16,8,2]{0,2,1:T(2,128)S(1)}, ...), condition=%wide.region_6.7_spmd, body=%wide.region_5.6_spmd.sunk | while | flops 99845 | bytes 669847 | solution.py:18
  82.8 0.1 copy.74
  83.0 0.1 copy.75
  83.1 0.8 fusion.37
  84.0 0.1 copy.74
  84.1 0.1 copy.75
  84.3 0.8 fusion.37
  85.1 0.1 copy.74
  85.2 0.1 copy.75
  85.4 0.8 fusion.37
  86.2 0.1 copy.43
  86.3 0.2 broadcast_divide_fusion
  86.5 0.2 slice_reduce_fusion
  86.8 0.0 copy-done.1
  86.8 0.2 multiply_reduce_fusion
  87.0 0.0 copy-done.2
  87.0 0.1 broadcast_bitcast_fusion
  87.1 0.1 mul.197
  87.1 2.6 %fusion.21 = f32[16,1024]{1,0:T(8,128)} fusion(bf16[1024,1024]{1,0:T(8,128)(2,1)} %param.16, f32[2,8,8,128]{3,2,1,0:T(8,128)S(1)} %bitcast.74, f32[2,8,8,128]{3,2,1,0:T(8,128)S(1)} %bitcast.73, f32[2,8,8,128]{3,2,1,0:T(8,128)S(1)} %bitcast.70, f32[1024]{0:T(1024)S(1)} %get-tuple-element.234, f32[1024]{0:T(1024)S(1)} %get-tuple-element.235), kind=kOutput, calls=%fused_computation.37 | convolution fusion | flops 33636352 | bytes 2367488 | tf_op jit(solution)/shard_map/dot_general | solution.py:98
  89.7 0.0 reduce-scatter.2.cloned.1.call-update
  89.8 5.9 %reduce-scatter.2.cloned.1.call-done = f32[16,512]{1,0:T(8,128)} async-done(((f32[16,1024]{1,0:T(8,128)}), f32[16,512]{1,0:T(8,128)}) %reduce-scatter.2.cloned.1.call-update) | async-done | bytes 32784 | tf_op jit(solution)/shard_map/reduce_scatter | solution.py:99
  95.7 1.4 %convert_element_type.24 = bf16[16,512]{1,0:T(8,128)(2,1)} convert(f32[16,512]{1,0:T(8,128)} %reduce-scatter.2.cloned.1.call-done) | non-fusion elementwise | flops 8192 | bytes 49152 | tf_op jit(solution)/shard_map/convert_element_type | solution.py:99
  (15 shorter events, 0.2 us)
Async XLA Ops:
  6.5 1.6 %copy-start = (bf16[1024,1024]{1,0:T(8,128)(2,1)S(1)}, bf16[1024,1024]{1,0:T(8,128)(2,1)}, u32[]{:S(2)}) copy-start(bf16[1024,1024]{1,0:T(8,128)(2,1)} %param.13) | copy-start | bytes 6291460
  6.5 31.2 %copy-start.3 = (s32[16]{0:T(128)S(1)}, s32[16]{0:T(128)}, u32[]{:S(2)}) copy-start(s32[16]{0:T(128)} %param.19) | copy-start | bytes 196
  6.5 89.2 %reduce-scatter.2.cloned.1.call-start = ((), (), s32[]{:S(2)}) async-start(), calls=%async_computation.1 | async-start | bytes 98304 | tf_op jit(solution)/shard_map/reduce_scatter | solution.py:99
  39.3 14.6 %copy-start.4 = (bf16[16,256,128]{2,1,0:T(8,128)(2,1)S(1)}, bf16[16,256,128]{2,1,0:T(8,128)(2,1)}, u32[]{:S(2)}) copy-start(bf16[16,256,128]{2,1,0:T(8,128)(2,1)} %param.18) | copy-start | bytes 3145732
  82.8 4.0 %copy-start.1 = (f32[8]{0:T(128)S(1)}, f32[8]{0:T(128)}, u32[]{:S(2)}) copy-start(f32[8]{0:T(128)} %param.14) | copy-start | bytes 100
  82.8 4.2 %copy-start.2 = (f32[128]{0:T(128)S(1)}, f32[128]{0:T(128)}, u32[]{:S(2)}) copy-start(f32[128]{0:T(128)} %param.15) | copy-start | bytes 1540
Sparse Core Ops, SparseCore 0:
  89.9 5.7 reduce-scatter.1
